TPU v7x, 128 devices: a whole 4x4x4 slice. The times are simulated.
128 devices in a mesh: tp: 16 (over z, x), dp: 8 (over y, core).
Axes of the slice: x: 4, y: 4, z: 4, core: 2. Of those that a mesh axis runs over, the one named last changes fastest.
Arguments:
- stream_in: bfloat16 [256, 4096], P('tp', 'dp'), may hold values from -21 to 21
- hidden_state: float32 [2, 256, 4096], P(None, 'dp', 'tp'), may hold values from -6 to 6
- convolution_window_state: bfloat16 [2, 256, 3, 4096], P(None, 'dp', None, 'tp'), may hold values from -6 to 6
- norm_gain: float32 [2, 4096], P(None, 'dp'), may hold values from 0.1 to 1.9
- path_weight: bfloat16 [2, 4096, 4096], P(None, 'dp', 'tp'), may hold values from -0.09375 to 0.09375
- output_gate_weight: bfloat16 [2, 4096, 4096], P(None, 'dp', 'tp'), may hold values from -0.09375 to 0.09375
- conv_taps: float32 [2, 4, 4096], P(None, None, 'tp'), may hold values from -3 to 3
- recur_map: float32 [2, 64, 64, 64], P(None, 'tp'), may hold values from -0.75 to 0.75
- input_map: float32 [2, 64, 64, 64], P(None, 'tp'), may hold values from -0.75 to 0.75
- decay_logit: float32 [2, 4096], P(None, 'tp'), may hold values from 1 to 6
- out_weight: bfloat16 [2, 4096, 4096], P(None, 'tp', 'dp'), may hold values from -0.09375 to 0.09375
Outputs:
- stream_out: bfloat16 [256, 4096], P('tp', 'dp')
- hidden_next: float32 [2, 256, 4096], P(None, 'dp', 'tp')
- conv_next: bfloat16 [2, 256, 3, 4096], P(None, 'dp', None, 'tp')
All inputs are finite; a program needn't handle non-finite values.
Results may differ from a plain program's by a relative error of at most 0.019.
Values may be sent and summed in bfloat16 or wider, within the bound.
A program may use at most 64 MiB of HBM per device.

v0:
```python
import jax
import jax.numpy as jnp
from jax import lax
from jax.sharding import PartitionSpec as P

D = 4096
TAPS = 4


EPS = 1e-06


def from_everyone(array, axis):
    copies = jnp.broadcast_to(array, (lax.axis_size(axis), *array.shape))
    return lax.all_to_all(copies, axis, split_axis=0, concat_axis=0, tiled=True)


def of_everyone(array, axis):
    everything = from_everyone(array, axis)
    return jnp.sum(everything, axis=0)


def in_order(parts, dim):
    parts = jnp.moveaxis(parts, 0, dim)
    shape = parts.shape
    return parts.reshape(*shape[:dim], shape[dim] * shape[dim + 1], *shape[dim + 2 :])


def collect(array, axis, dim):
    return in_order(from_everyone(array, axis), dim)


def in_blocks(array, dim, devices):
    before, after = (array.shape[:dim], array.shape[dim + 1 :])
    return jnp.moveaxis(array.reshape(*before, devices, -1, *after), dim, 0)


def sum_at_owner(array, axis, dim):
    parts = in_blocks(array, dim, lax.axis_size(axis))
    arrived = lax.all_to_all(parts, axis, split_axis=0, concat_axis=0, tiled=True)
    return arrived.astype(jnp.float32).sum(axis=0)


def scaled(rows, gain):
    rowsf = rows.astype(jnp.float32)
    sumsq = of_everyone(jnp.sum(rowsf * rowsf, axis=1), "dp")
    return (rowsf * lax.rsqrt(sumsq / D + EPS)[:, None] * gain[None, :]).astype(jnp.bfloat16)


def shard_inputs(normed, path_w, gate_branch_matrix):
    return jnp.concatenate(
        [
            jnp.dot(normed, path_w, preferred_element_type=jnp.float32),
            jnp.dot(normed, gate_branch_matrix, preferred_element_type=jnp.float32),
        ],
        axis=1,
    )


def split_inputs(rows, gain, path_w, gate_branch_matrix):
    normed = scaled(rows, gain)
    return shard_inputs(collect(normed, "tp", 0), path_w, gate_branch_matrix)


def recur_tail(partial_value, hidden, buffer, taps, recur_w, input_matrix, logit, out_w):
    width = partial_value.shape[1] // 2
    summed = sum_at_owner(partial_value.astype(jnp.bfloat16), "dp", 0)
    zpath = summed[:, :width].astype(jnp.bfloat16)
    zgate = summed[:, width:].astype(jnp.bfloat16)
    batch = zpath.shape[0]
    conv = zpath.astype(jnp.float32) * taps[TAPS - 1][None, :]
    for j in range(TAPS - 1):
        conv = conv + buffer[:, j].astype(jnp.float32) * taps[j][None, :]
    new_buffer = jnp.concatenate([buffer[:, 1:], zpath[:, None, :]], axis=1)
    cblocks = conv.reshape(batch, recur_w.shape[0], recur_w.shape[1])
    rgate = jax.nn.sigmoid(
        jnp.einsum("bnc,ncd->bnd", cblocks, recur_w, precision=lax.Precision.HIGHEST).reshape(
            batch, width
        )
    )
    igate = jax.nn.sigmoid(
        jnp.einsum("bnc,ncd->bnd", cblocks, input_matrix, precision=lax.Precision.HIGHEST).reshape(
            batch, width
        )
    )
    loga = 8.0 * rgate * jax.nn.log_sigmoid(logit)[None, :]
    new_hidden = jnp.exp(loga) * hidden + jnp.sqrt(-jnp.expm1(2.0 * loga)) * (igate * conv)
    mixed = (new_hidden * jax.nn.gelu(zgate.astype(jnp.float32))).astype(jnp.bfloat16)
    update = jnp.dot(collect(mixed, "dp", 0), out_w, preferred_element_type=jnp.float32)
    return (update, new_hidden, new_buffer)


def per_device(
    stream_in,
    hidden_state,
    convolution_window_state,
    norm_gain,
    path_weight,
    output_gate_weight,
    conv_taps,
    recur_map,
    input_map,
    decay_logit,
    out_weight,
):
    stream = stream_in
    partial_value = split_inputs(stream, norm_gain[0], path_weight[0], output_gate_weight[0])
    update, hidden_first, buffer_first = recur_tail(
        partial_value,
        hidden_state[0],
        convolution_window_state[0],
        conv_taps[0],
        recur_map[0],
        input_map[0],
        decay_logit[0],
        out_weight[0],
    )
    stream = (
        stream.astype(jnp.float32) + sum_at_owner(update.astype(jnp.bfloat16), "tp", 0)
    ).astype(jnp.bfloat16)
    partial_value = split_inputs(stream, norm_gain[1], path_weight[1], output_gate_weight[1])
    update, hidden_second, buffer_second = recur_tail(
        partial_value,
        hidden_state[1],
        convolution_window_state[1],
        conv_taps[1],
        recur_map[1],
        input_map[1],
        decay_logit[1],
        out_weight[1],
    )
    stream = (
        stream.astype(jnp.float32) + sum_at_owner(update.astype(jnp.bfloat16), "tp", 0)
    ).astype(jnp.bfloat16)
    return (
        stream,
        jnp.stack([hidden_first, hidden_second]),
        jnp.stack([buffer_first, buffer_second]),
    )


def solution(mesh):
    placed = (
        P("tp", "dp"),
        P(None, "dp", "tp"),
        P(None, "dp", None, "tp"),
        P(None, "dp"),
        P(None, "dp", "tp"),
        P(None, "dp", "tp"),
        P(None, None, "tp"),
        P(None, "tp", None, None),
        P(None, "tp", None, None),
        P(None, "tp"),
        P(None, "tp", "dp"),
    )
    return jax.shard_map(
        per_device,
        mesh=mesh,
        in_specs=placed,
        out_specs=(P("tp", "dp"), P(None, "dp", "tp"), P(None, "dp", None, "tp")),
        check_vma=False,
    )
```

profile of v0, /device:TPU:1, one launch (start us, length us, event | category | flops | bytes accessed | tf_op | source)
XLA Modules:
  0.0 123.0 jit_solution(2130089506699500946)
XLA Ops:
  0.6 0.0 copy-start
  0.6 0.9 fusion.40
  1.5 0.6 broadcast_in_dim.28
  2.1 6.0 %all-to-all-start = ((f32[8,1,16]{2,1,0:T(1,128)}), f32[8,1,16]{2,1,0:T(1,128)S(1)}, u32[]{:S(2)}, u32[]{:S(2)}) async-start(f32[8,1,16]{2,1,0:T(1,128)} %broadcast_in_dim.28), calls=%async_computation | async-start | bytes 8192 | tf_op jit(solution)/shard_map/all_to_all | solution.py:15
  8.1 0.8 fusion.78
  8.9 3.8 %all-to-all-done = f32[8,1,16]{2,1,0:T(1,128)S(1)} async-done(((f32[8,1,16]{2,1,0:T(1,128)}), f32[8,1,16]{2,1,0:T(1,128)S(1)}, u32[]{:S(2)}, u32[]{:S(2)}) %all-to-all-start) | async-done | bytes 544 | tf_op jit(solution)/shard_map/all_to_all | solution.py:15
  12.6 0.8 fusion.42
  13.4 0.0 copy-start.6
  13.4 0.7 broadcast_in_dim.29
  14.2 7.7 %all-to-all-start.1 = ((bf16[16,16,512]{2,1,0:T(8,128)(2,1)}), bf16[16,16,512]{2,1,0:T(8,128)(2,1)S(1)}, u32[]{:S(2)}, u32[]{:S(2)}) async-start(bf16[16,16,512]{2,1,0:T(8,128)(2,1)} %broadcast_in_dim.29), calls=%async_computation.1 | async-start | bytes 524288 | tf_op jit(solution)/shard_map/all_to_all | solution.py:15
  21.9 0.0 copy-done.6
  21.9 7.5 %all-to-all-done.1 = bf16[16,16,512]{2,1,0:T(8,128)(2,1)S(1)} async-done(((bf16[16,16,512]{2,1,0:T(8,128)(2,1)}), bf16[16,16,512]{2,1,0:T(8,128)(2,1)S(1)}, u32[]{:S(2)}, u32[]{:S(2)}) %all-to-all-start.1) | async-done | bytes 262176 | tf_op jit(solution)/shard_map/all_to_all | solution.py:15
  29.5 0.0 copy-done
  29.5 0.2 convolution_convert_fusion.4
  29.7 0.0 copy-done.1
  29.7 0.2 convolution_convert_fusion.5
  29.9 0.7 pad_maximum_fusion
  30.7 5.6 %all-to-all-start.2 = ((bf16[8,32,512]{2,1,0:T(8,128)(2,1)}), bf16[8,32,512]{2,1,0:T(8,128)(2,1)S(1)}, u32[]{:S(2)}, u32[]{:S(2)}) async-start(bf16[8,32,512]{2,1,0:T(8,128)(2,1)} %pad_maximum_fusion), calls=%async_computation.2 | async-start | bytes 524288 | tf_op jit(solution)/shard_map/all_to_all | solution.py:40
  36.2 0.0 copy-done.7
  36.3 0.0 copy-done.4
  36.3 0.0 copy-start.8
  36.3 6.4 %all-to-all-done.2 = bf16[8,32,512]{2,1,0:T(8,128)(2,1)S(1)} async-done(((bf16[8,32,512]{2,1,0:T(8,128)(2,1)}), bf16[8,32,512]{2,1,0:T(8,128)(2,1)S(1)}, u32[]{:S(2)}, u32[]{:S(2)}) %all-to-all-start.2) | async-done | bytes 262176 | tf_op jit(solution)/shard_map/all_to_all | solution.py:40
  42.8 0.0 copy-start.9
  42.8 0.1 reshape.118
  42.9 0.0 copy-done.8
  42.9 0.2 fusion.11
  43.2 0.6 copy-done.9
  43.7 0.2 fusion.15
  44.0 0.0 copy-start.2
  44.0 0.1 div.32
  44.2 0.1 div.34
  44.3 0.3 copy-done.5
  44.6 0.1 fusion.54
  44.6 8.7 %all_to_all.52 = bf16[8,32,256]{2,1,0:T(8,128)(2,1)S(1)} all-to-all(bf16[8,32,256]{2,1,0:T(8,128)(2,1)S(1)} %broadcast_in_dim.30), channel_id=1, replica_groups=mesh['tp'=16,'dp'=8] {'dp'}, dimensions={0} | all-to-all | bytes 262144 | tf_op jit(solution)/shard_map/all_to_all | solution.py:15
  53.3 0.0 copy-done.2
  53.3 0.2 convolution_convert_fusion.1
  53.5 10.2 %all_to_all.53 = bf16[16,16,512]{2,1,0:T(8,128)(2,1)S(1)} all-to-all(bf16[16,16,512]{2,1,0:T(8,128)(2,1)S(1)} %bitcast.126), channel_id=1, replica_groups=mesh['tp'=16,'dp'=8] {'tp'}, dimensions={0} | all-to-all | bytes 524288 | tf_op jit(solution)/shard_map/all_to_all | solution.py:40
  63.8 0.7 copy-done.3
  64.4 0.1 fusion.44
  64.6 9.2 %all_to_all.54 = f32[8,1,16]{2,1,0:T(1,128)S(1)} all-to-all(f32[8,1,16]{2,1,0:T(1,128)S(1)} %broadcast_in_dim.31), channel_id=1, replica_groups=mesh['tp'=16,'dp'=8] {'dp'}, dimensions={0} | all-to-all | bytes 1024 | tf_op jit(solution)/shard_map/all_to_all | solution.py:15
  73.8 0.1 fusion.46
  73.9 0.7 broadcast_in_dim.32
  74.6 3.5 %all-to-all-start.6 = ((bf16[16,16,512]{2,1,0:T(8,128)(2,1)}), bf16[16,16,512]{2,1,0:T(8,128)(2,1)S(1)}, u32[]{:S(2)}, u32[]{:S(2)}) async-start(bf16[16,16,512]{2,1,0:T(8,128)(2,1)} %broadcast_in_dim.32), calls=%async_computation.6 | async-start | bytes 524288 | tf_op jit(solution)/shard_map/all_to_all | solution.py:15
  78.2 8.0 %all-to-all-done.6 = bf16[16,16,512]{2,1,0:T(8,128)(2,1)S(1)} async-done(((bf16[16,16,512]{2,1,0:T(8,128)(2,1)}), bf16[16,16,512]{2,1,0:T(8,128)(2,1)S(1)}, u32[]{:S(2)}, u32[]{:S(2)}) %all-to-all-start.6) | async-done | bytes 262176 | tf_op jit(solution)/shard_map/all_to_all | solution.py:15
  86.2 0.2 convolution_convert_fusion.2
  86.4 0.2 convolution_convert_fusion.3
  86.7 0.7 pad_maximum_fusion.1
  87.4 4.9 %all-to-all-start.7 = ((bf16[8,32,512]{2,1,0:T(8,128)(2,1)}), bf16[8,32,512]{2,1,0:T(8,128)(2,1)S(1)}, u32[]{:S(2)}, u32[]{:S(2)}) async-start(bf16[8,32,512]{2,1,0:T(8,128)(2,1)} %pad_maximum_fusion.1), calls=%async_computation.7 | async-start | bytes 524288 | tf_op jit(solution)/shard_map/all_to_all | solution.py:40
  92.3 6.5 %all-to-all-done.7 = bf16[8,32,512]{2,1,0:T(8,128)(2,1)S(1)} async-done(((bf16[8,32,512]{2,1,0:T(8,128)(2,1)}), bf16[8,32,512]{2,1,0:T(8,128)(2,1)S(1)}, u32[]{:S(2)}, u32[]{:S(2)}) %all-to-all-start.7) | async-done | bytes 262176 | tf_op jit(solution)/shard_map/all_to_all | solution.py:40
  98.8 0.1 reshape.121
  98.9 0.2 fusion.3
  99.2 0.2 fusion.7
  99.5 0.1 div.37
  99.6 0.1 div.39
  99.7 0.1 fusion.61
  99.8 0.7 broadcast_in_dim.33
  100.5 4.3 %all-to-all-start.8 = ((bf16[8,32,256]{2,1,0:T(8,128)(2,1)}), bf16[8,32,256]{2,1,0:T(8,128)(2,1)S(1)}, u32[]{:S(2)}, u32[]{:S(2)}) async-start(bf16[8,32,256]{2,1,0:T(8,128)(2,1)} %broadcast_in_dim.33), calls=%async_computation.8 | async-start | bytes 262144 | tf_op jit(solution)/shard_map/all_to_all | solution.py:15
  104.8 5.3 %all-to-all-done.8 = bf16[8,32,256]{2,1,0:T(8,128)(2,1)S(1)} async-done(((bf16[8,32,256]{2,1,0:T(8,128)(2,1)}), bf16[8,32,256]{2,1,0:T(8,128)(2,1)S(1)}, u32[]{:S(2)}, u32[]{:S(2)}) %all-to-all-start.8) | async-done | bytes 131104 | tf_op jit(solution)/shard_map/all_to_all | solution.py:15
  110.0 0.9 convolution_convert_fusion
  111.0 3.5 %all-to-all-start.9 = ((bf16[16,16,512]{2,1,0:T(8,128)(2,1)}), bf16[16,16,512]{2,1,0:T(8,128)(2,1)S(1)}, u32[]{:S(2)}, u32[]{:S(2)}) async-start(bf16[16,16,512]{2,1,0:T(8,128)(2,1)} %bitcast.47), calls=%async_computation.9 | async-start | bytes 524288 | tf_op jit(solution)/shard_map/all_to_all | solution.py:40
  114.5 0.6 pad_maximum_fusion.3
  115.2 0.7 pad_maximum_fusion.2
  115.8 6.6 %all-to-all-done.9 = bf16[16,16,512]{2,1,0:T(8,128)(2,1)S(1)} async-done(((bf16[16,16,512]{2,1,0:T(8,128)(2,1)}), bf16[16,16,512]{2,1,0:T(8,128)(2,1)S(1)}, u32[]{:S(2)}, u32[]{:S(2)}) %all-to-all-start.9) | async-done | bytes 262176 | tf_op jit(solution)/shard_map/all_to_all | solution.py:40
  122.4 0.6 fusion.47
  (30 shorter events, 0.5 us)
Async XLA Ops:
  0.6 28.8 %copy-start = (bf16[2,512,256]{2,1,0:T(8,128)(2,1)S(1)}, bf16[2,512,256]{2,1,0:T(8,128)(2,1)}, u32[]{:S(2)}) copy-start(bf16[2,512,256]{2,1,0:T(8,128)(2,1)} %param.16) | copy-start | bytes 1572868
  2.1 10.5 %all-to-all-start = ((f32[8,1,16]{2,1,0:T(1,128)}), f32[8,1,16]{2,1,0:T(1,128)S(1)}, u32[]{:S(2)}, u32[]{:S(2)}) async-start(f32[8,1,16]{2,1,0:T(1,128)} %broadcast_in_dim.28), calls=%async_computation | async-start | bytes 8192 | tf_op jit(solution)/shard_map/all_to_all | solution.py:15
  13.4 8.5 %copy-start.6 = (f32[2,4,256]{2,1,0:T(4,128)S(1)}, f32[2,4,256]{2,1,0:T(4,128)}, u32[]{:S(2)}) copy-start(f32[2,4,256]{2,1,0:T(4,128)} %param.17) | copy-start | bytes 24580
  14.2 15.5 %copy-start.1 = (bf16[2,512,256]{2,1,0:T(8,128)(2,1)S(1)}, bf16[2,512,256]{2,1,0:T(8,128)(2,1)}, u32[]{:S(2)}) copy-start(bf16[2,512,256]{2,1,0:T(8,128)(2,1)} %param.15) | copy-start | bytes 1572868
  14.2 15.3 %all-to-all-start.1 = ((bf16[16,16,512]{2,1,0:T(8,128)(2,1)}), bf16[16,16,512]{2,1,0:T(8,128)(2,1)S(1)}, u32[]{:S(2)}, u32[]{:S(2)}) async-start(bf16[16,16,512]{2,1,0:T(8,128)(2,1)} %broadcast_in_dim.29), calls=%async_computation.1 | async-start | bytes 524288 | tf_op jit(solution)/shard_map/all_to_all | solution.py:15
  30.7 5.6 %copy-start.7 = (f32[2,256]{1,0:T(2,128)S(1)}, f32[2,256]{1,0:T(2,128)}, u32[]{:S(2)}) copy-start(f32[2,256]{1,0:T(2,128)} %param.20) | copy-start | bytes 6148
  30.7 5.6 %copy-start.4 = (bf16[2,32,3,256]{3,1,2,0:T(8,128)(2,1)S(1)}, bf16[2,32,3,256]{3,1,2,0:T(8,128)(2,1)}, u32[]{:S(2)}) copy-start(bf16[2,32,3,256]{3,1,2,0:T(8,128)(2,1)} %param.13) | copy-start | bytes 294916
  30.7 12.1 %all-to-all-start.2 = ((bf16[8,32,512]{2,1,0:T(8,128)(2,1)}), bf16[8,32,512]{2,1,0:T(8,128)(2,1)S(1)}, u32[]{:S(2)}, u32[]{:S(2)}) async-start(bf16[8,32,512]{2,1,0:T(8,128)(2,1)} %pad_maximum_fusion), calls=%async_computation.2 | async-start | bytes 524288 | tf_op jit(solution)/shard_map/all_to_all | solution.py:40
  36.3 6.6 %copy-start.8 = (f32[2,4,64,64]{3,2,1,0:T(8,128)S(1)}, f32[2,4,64,64]{3,2,1,0:T(8,128)}, u32[]{:S(2)}) copy-start(f32[2,4,64,64]{3,2,1,0:T(8,128)} %param.19) | copy-start | bytes 393220
  42.8 1.0 copy-start.9
  43.7 0.8 copy-start.5
  44.0 9.3 %copy-start.2 = (bf16[2,256,512]{2,1,0:T(8,128)(2,1)S(1)}, bf16[2,256,512]{2,1,0:T(8,128)(2,1)}, u32[]{:S(2)}) copy-start(bf16[2,256,512]{2,1,0:T(8,128)(2,1)} %param.21) | copy-start | bytes 1572868
  63.7 0.7 copy-start.3
  74.6 11.6 %all-to-all-start.6 = ((bf16[16,16,512]{2,1,0:T(8,128)(2,1)}), bf16[16,16,512]{2,1,0:T(8,128)(2,1)S(1)}, u32[]{:S(2)}, u32[]{:S(2)}) async-start(bf16[16,16,512]{2,1,0:T(8,128)(2,1)} %broadcast_in_dim.32), calls=%async_computation.6 | async-start | bytes 524288 | tf_op jit(solution)/shard_map/all_to_all | solution.py:15
  87.4 11.4 %all-to-all-start.7 = ((bf16[8,32,512]{2,1,0:T(8,128)(2,1)}), bf16[8,32,512]{2,1,0:T(8,128)(2,1)S(1)}, u32[]{:S(2)}, u32[]{:S(2)}) async-start(bf16[8,32,512]{2,1,0:T(8,128)(2,1)} %pad_maximum_fusion.1), calls=%async_computation.7 | async-start | bytes 524288 | tf_op jit(solution)/shard_map/all_to_all | solution.py:40
  100.5 9.6 %all-to-all-start.8 = ((bf16[8,32,256]{2,1,0:T(8,128)(2,1)}), bf16[8,32,256]{2,1,0:T(8,128)(2,1)S(1)}, u32[]{:S(2)}, u32[]{:S(2)}) async-start(bf16[8,32,256]{2,1,0:T(8,128)(2,1)} %broadcast_in_dim.33), calls=%async_computation.8 | async-start | bytes 262144 | tf_op jit(solution)/shard_map/all_to_all | solution.py:15
  111.0 11.4 %all-to-all-start.9 = ((bf16[16,16,512]{2,1,0:T(8,128)(2,1)}), bf16[16,16,512]{2,1,0:T(8,128)(2,1)S(1)}, u32[]{:S(2)}, u32[]{:S(2)}) async-start(bf16[16,16,512]{2,1,0:T(8,128)(2,1)} %bitcast.47), calls=%async_computation.9 | async-start | bytes 524288 | tf_op jit(solution)/shard_map/all_to_all | solution.py:40
where the time goes:
time: 125 us; the launch traced here: 123 us
  waiting for transfers between devices  44.1 us (35%)
  starting transfers between devices  35.5 us (28%)
  blocking collectives  28.1 us (22%)
  local copies, waits for them, and re-layouts  5.85 us (5%)
  other arithmetic  5.62 us (4%)
  matrix products  3.06 us (2%)
    all_to_all x4, waiting for transfers between devices, from_everyone(): return lax.all_to_all(copies, axis, split_axis=0, concat_axis=0, tiled=True)  24.6 us
    all_to_all x4, starting transfers between devices, from_everyone(): return lax.all_to_all(copies, axis, split_axis=0, concat_axis=0, tiled=True)  21.5 us
    all_to_all x3, waiting for transfers between devices, sum_at_owner(): lax.all_to_all(parts, axis, split_axis=0, concat_axis=0, tiled=True)  19.5 us
    all_to_all x2, blocking collectives, from_everyone(): return lax.all_to_all(copies, axis, split_axis=0, concat_axis=0, tiled=True)  17.9 us
    all_to_all x3, starting transfers between devices, sum_at_owner(): lax.all_to_all(parts, axis, split_axis=0, concat_axis=0, tiled=True)  14 us
    all_to_all x1, blocking collectives, sum_at_owner(): lax.all_to_all(parts, axis, split_axis=0, concat_axis=0, tiled=True)  10.2 us
    broadcast_in_dim x6, local copies, waits for them, and re-layouts, from_everyone(): copies = jnp.broadcast_to(array, (lax.axis_size(axis), *array.shape))  2.74 us
  transfers between devices with their start and end apart: 7, of which 7 were waited for; matrix products, arithmetic and copies ran while one was open for 2% of the time, Pallas kernels for 0%

commit v1 on v0

v1 whole, which is shorter than its diff:
```python
import functools

import jax
import jax.numpy as jnp
from jax import lax
from jax.experimental import pallas as pl
from jax.experimental.pallas import tpu as pltpu
from jax.sharding import PartitionSpec as P

D = 4096
TAPS = 4
EPS = 1e-06
LAYERS = 2
NZ, NX, NY, NC = 4, 4, 4, 2
TP, DP = NZ * NX, NY * NC
ROWS = 16
SROWS = 32
DLOC = 512
W = 256
MESH = pl.DeviceIdType.MESH
f32, bf16 = jnp.float32, jnp.bfloat16


def near(k):
    half = lax.div(k, 2)
    return k + half * (1 - 2 * lax.rem(k, 2))


def kernel(x_h, hid_h, buf_h, gain_h, pw_h, gw_h, taps_h, rmap_h, imap_h, logit_h, ow_h,
           so_ref, ho_ref, bo_ref,
           xg, wz, wo, hid, buf, gain, taps, logit, rmap, imap, bdh, bdl, pre, la,
           zs, zr, sss, ssr, ms, mg, us, ur,
           lsem, xss, xrs, zss, zrs, qss, qrs, mss, mrs, uss, urs):
    tp = lax.axis_index("tp")
    dp = lax.axis_index("dp")
    z0, x0 = lax.div(tp, NX), lax.rem(tp, NX)
    y0, c0 = lax.div(dp, NC), lax.rem(dp, NC)

    def tp_at(i):
        z = lax.rem(z0 + near(lax.div(i, 4)), NZ)
        x = lax.rem(x0 + near(lax.rem(i, 4)), NX)
        return z * NX + x

    def dp_at(i):
        y = lax.rem(y0 + near(lax.div(i, 2)), NY)
        c = lax.rem(c0 + lax.rem(i, 2), NC)
        return y * NC + c

    def group_at(i):
        z = lax.rem(z0 + near(lax.div(i, 2)), NZ)
        p = lax.rem(lax.div(x0, 2) + lax.rem(i, 2), 2)
        return z * 2 + p

    loads = [
        (x_h, xg.at[0, tp]),
        (gain_h, gain),
        (pw_h.at[0], wz.at[0, :, pl.ds(0, W)]),
        (gw_h.at[0], wz.at[0, :, pl.ds(W, W)]),
        (buf_h, buf),
        (taps_h, taps),
        (logit_h, logit),
        (rmap_h, rmap),
        (imap_h, imap),
        (hid_h, hid),
        (ow_h.at[0], wo.at[0]),
        (pw_h.at[1], wz.at[1, :, pl.ds(0, W)]),
        (gw_h.at[1], wz.at[1, :, pl.ds(W, W)]),
        (ow_h.at[1], wo.at[1]),
    ]
    copies = [pltpu.make_async_copy(a, b, lsem.at[i]) for i, (a, b) in enumerate(loads)]
    for c in copies:
        c.start()

    barrier = pltpu.get_barrier_semaphore()

    def greet_tp(i, _):
        pl.semaphore_signal(barrier, inc=1, device_id={"tp": tp_at(TP - i), "dp": dp}, device_id_type=MESH)
        return 0

    def greet_dp(i, _):
        pl.semaphore_signal(barrier, inc=1, device_id={"tp": tp, "dp": dp_at(DP - i)}, device_id_type=MESH)
        return 0

    lax.fori_loop(1, TP, greet_tp, 0)
    lax.fori_loop(1, DP, greet_dp, 0)

    for i in (4, 5, 6, 7, 8):
        copies[i].wait()
    la[...] = 8.0 * jax.nn.log_sigmoid(logit[...])
    for l in range(LAYERS):
        acc = buf[l, 0].astype(f32) * taps[l, 0:1, :]
        for j in range(1, TAPS - 1):
            acc = acc + buf[l, j].astype(f32) * taps[l, j : j + 1, :]
        pre[l] = acc
        bo_ref[l, 0] = buf[l, 1]
        bo_ref[l, 1] = buf[l, 2]
        zero = jnp.zeros((64, 64), f32)
        zpair = jnp.zeros((64, 128), bf16)
        for b in range(4):
            for m, ref in enumerate((rmap, imap)):
                block = ref[l, b]
                wide = jnp.concatenate([block, zero] if b % 2 == 0 else [zero, block], axis=1)
                hi = wide.astype(bf16)
                lo = (wide - hi.astype(f32)).astype(bf16)
                for h in range(2):
                    at = pl.ds(m * W + h * 128, 128)
                    here = h == b // 2
                    bdh[l, b * 64 : b * 64 + 64, at] = hi if here else zpair
                    bdl[l, b * 64 : b * 64 + 64, at] = lo if here else zpair

    copies[0].wait()
    pl.semaphore_wait(barrier, TP - 1 + DP - 1)

    def x_copy(l, t, slot):
        return pltpu.make_async_remote_copy(
            src_ref=xg.at[l, tp], dst_ref=xg.at[l, slot],
            send_sem=xss.at[l, t], recv_sem=xrs.at[l, slot],
            device_id={"tp": t, "dp": dp}, device_id_type=MESH)

    def z_copy(l, d, slot):
        return pltpu.make_async_remote_copy(
            src_ref=zs.at[l, d], dst_ref=zr.at[l, slot],
            send_sem=zss.at[l, d], recv_sem=zrs.at[l, slot],
            device_id={"tp": tp, "dp": d}, device_id_type=MESH)

    def q_copy(l, d, slot):
        return pltpu.make_async_remote_copy(
            src_ref=sss.at[l, d], dst_ref=ssr.at[l, slot],
            send_sem=qss.at[l, d], recv_sem=qrs.at[l, slot],
            device_id={"tp": tp, "dp": d}, device_id_type=MESH)

    def m_copy(l, d, slot):
        return pltpu.make_async_remote_copy(
            src_ref=ms.at[l], dst_ref=mg.at[l, slot],
            send_sem=mss.at[l, d], recv_sem=mrs.at[l, slot],
            device_id={"tp": tp, "dp": d}, device_id_type=MESH)

    def u_copy(l, t, slot):
        return pltpu.make_async_remote_copy(
            src_ref=us.at[l, t], dst_ref=ur.at[l, slot],
            send_sem=uss.at[l, t], recv_sem=urs.at[l, slot],
            device_id={"tp": t, "dp": dp}, device_id_type=MESH)

    eye = (lax.broadcasted_iota(jnp.int32, (SROWS, 128), 0)
           == lax.broadcasted_iota(jnp.int32, (SROWS, 128), 1))

    for l in range(LAYERS):
        def send_x(i, _):
            x_copy(l, tp_at(TP - i), tp).start()
            return 0

        lax.fori_loop(1, TP, send_x, 0)
        if l == 0:
            for i in (1, 2, 3):
                copies[i].wait()
        else:
            copies[11].wait()
            copies[12].wait()

        def project(i, _):
            g = group_at(i)
            for h in range(2):
                t = 2 * g + h

                @pl.when(t != tp)
                def _():
                    x_copy(l, t, t).wait_recv()

            xf = xg[l, pl.ds(2 * g, 2)].astype(f32).reshape(SROWS, DLOC)
            xn = (xf * gain[l : l + 1, :]).astype(bf16)
            zs[l, g] = jnp.dot(xn, wz[l], preferred_element_type=f32).astype(bf16)
            sq = xf * xf
            sq = (sq[:, 0:128] + sq[:, 128:256]) + (sq[:, 256:384] + sq[:, 384:512])
            tot = jnp.sum(sq, axis=1, keepdims=True)
            sss[l, g] = jnp.sum(jnp.where(eye, tot, 0.0), axis=0, keepdims=True)

            @pl.when(g != dp)
            def _():
                z_copy(l, g, dp).start()
                q_copy(l, g, dp).start()

            return 0

        lax.fori_loop(0, DP, project, 0)

        if l == 0:
            copies[9].wait()
        acc = zs[l, dp].astype(f32)
        ssum = sss[l, dp]
        for i in range(1, DP):
            d = dp_at(jnp.int32(i))
            z_copy(l, d, d).wait_recv()
            q_copy(l, d, d).wait_recv()
            acc = acc + zr[l, d].astype(f32)
            ssum = ssum + ssr[l, d]
        ss = jnp.sum(jnp.where(eye, ssum, 0.0), axis=1, keepdims=True)
        acc = acc * lax.rsqrt(ss / D + EPS)
        zp = acc[:, :W].astype(bf16)
        zg = acc[:, W:].astype(bf16).astype(f32)

        conv = pre[l] + zp.astype(f32) * taps[l, TAPS - 1 : TAPS, :]
        ch = conv.astype(bf16)
        cl = (conv - ch.astype(f32)).astype(bf16)
        gates = (jnp.dot(ch, bdh[l], preferred_element_type=f32)
                 + jnp.dot(cl, bdh[l], preferred_element_type=f32)
                 + jnp.dot(ch, bdl[l], preferred_element_type=f32))
        rg = jax.nn.sigmoid(gates[:, :W])
        ig = jax.nn.sigmoid(gates[:, W:])
        loga = rg * la[l : l + 1, :]
        th = jnp.tanh(loga)
        hn = jnp.exp(loga) * hid[l] + jnp.sqrt(-2.0 * th / (1.0 - th)) * (ig * conv)
        ms[l] = (hn * jax.nn.gelu(zg)).astype(bf16)

        def send_m(i, _):
            m_copy(l, dp_at(DP - i), dp).start()
            return 0

        lax.fori_loop(1, DP, send_m, 0)
        ho_ref[l] = hn
        bo_ref[l, 2] = zp
        copies[10 if l == 0 else 13].wait()

        def emit(d, rows):
            u = jnp.dot(rows, wo[l], preferred_element_type=f32).astype(bf16)
            us[l, pl.ds(2 * d, 2)] = u.reshape(2, ROWS, DLOC)
            for h in range(2):
                t = 2 * d + h

                @pl.when(t != tp)
                def _():
                    u_copy(l, t, tp).start()

        emit(dp, ms[l])

        def update(i, _):
            d = dp_at(i)
            m_copy(l, d, d).wait_recv()
            emit(d, mg[l, d])
            return 0

        lax.fori_loop(1, DP, update, 0)

        acc = xg[l, tp].astype(f32)
        upd = us[l, tp].astype(f32)
        for i in range(1, TP):
            t = tp_at(jnp.int32(i))
            u_copy(l, t, t).wait_recv()
            upd = upd + ur[l, t].astype(f32)
        out = (acc + upd).astype(bf16)
        if l + 1 < LAYERS:
            xg[l + 1, tp] = out
        else:
            so_ref[...] = out

    for l in range(LAYERS):
        def drain_tp(i, _):
            t = tp_at(i)
            x_copy(l, t, tp).wait_send()
            u_copy(l, t, tp).wait_send()
            return 0

        def drain_dp(i, _):
            d = dp_at(i)
            z_copy(l, d, dp).wait_send()
            q_copy(l, d, dp).wait_send()
            m_copy(l, d, dp).wait_send()
            return 0

        lax.fori_loop(1, TP, drain_tp, 0)
        lax.fori_loop(1, DP, drain_dp, 0)


def per_device(*args):
    args = list(args)
    args[2] = jnp.transpose(args[2], (0, 2, 1, 3))
    V = pltpu.VMEM
    S = pltpu.SemaphoreType.DMA
    so, ho, bo = pl.pallas_call(
        kernel,
        out_shape=(
            jax.ShapeDtypeStruct((ROWS, DLOC), bf16),
            jax.ShapeDtypeStruct((LAYERS, SROWS, W), f32),
            jax.ShapeDtypeStruct((LAYERS, TAPS - 1, SROWS, W), bf16),
        ),
        in_specs=[pl.BlockSpec(memory_space=pltpu.HBM)] * 11,
        out_specs=[pl.BlockSpec(memory_space=pltpu.VMEM)] * 3,
        scratch_shapes=[
            V((LAYERS, TP, ROWS, DLOC), bf16),
            V((LAYERS, DLOC, 2 * W), bf16),
            V((LAYERS, W, DLOC), bf16),
            V((LAYERS, SROWS, W), f32),
            V((LAYERS, TAPS - 1, SROWS, W), bf16),
            V((LAYERS, DLOC), f32),
            V((LAYERS, TAPS, W), f32),
            V((LAYERS, W), f32),
            V((LAYERS, 4, 64, 64), f32),
            V((LAYERS, 4, 64, 64), f32),
            V((LAYERS, W, 2 * W), bf16),
            V((LAYERS, W, 2 * W), bf16),
            V((LAYERS, SROWS, W), f32),
            V((LAYERS, W), f32),
            V((LAYERS, DP, SROWS, 2 * W), bf16),
            V((LAYERS, DP, SROWS, 2 * W), bf16),
            V((LAYERS, DP, 1, 128), f32),
            V((LAYERS, DP, 1, 128), f32),
            V((LAYERS, SROWS, W), bf16),
            V((LAYERS, DP, SROWS, W), bf16),
            V((LAYERS, TP, ROWS, DLOC), bf16),
            V((LAYERS, TP, ROWS, DLOC), bf16),
            S((14,)),
            S((LAYERS, TP)), S((LAYERS, TP)),
            S((LAYERS, DP)), S((LAYERS, DP)),
            S((LAYERS, DP)), S((LAYERS, DP)),
            S((LAYERS, DP)), S((LAYERS, DP)),
            S((LAYERS, TP)), S((LAYERS, TP)),
        ],
        compiler_params=pltpu.CompilerParams(
            collective_id=0, has_side_effects=True, vmem_limit_bytes=40 * 1024 * 1024),
        name="blocks",
    )(*args)
    return so, ho, jnp.transpose(bo, (0, 2, 1, 3))


def solution(mesh):
    placed = (
        P("tp", "dp"),
        P(None, "dp", "tp"),
        P(None, "dp", None, "tp"),
        P(None, "dp"),
        P(None, "dp", "tp"),
        P(None, "dp", "tp"),
        P(None, None, "tp"),
        P(None, "tp", None, None),
        P(None, "tp", None, None),
        P(None, "tp"),
        P(None, "tp", "dp"),
    )
    return jax.shard_map(
        per_device,
        mesh=mesh,
        in_specs=placed,
        out_specs=(P("tp", "dp"), P(None, "dp", "tp"), P(None, "dp", None, "tp")),
        check_vma=False,
    )
```

time: 125 us -> 63.6 us (0.51)
  the two profiles are of different devices: /device:TPU:1 before, /device:TPU:8 now
where the time goes in v1:
time: 63.6 us; the launch traced here: 63 us
  Pallas kernels  51 us (80%)
  local copies, waits for them, and re-layouts  11.4 us (18%)
  between operations  0.66 us (1%)
    pallas_call x1, Pallas kernels, per_device(): pl.pallas_call(kernel, out_shape=(jax.ShapeDtypeStruct((ROWS, DLOC), bf16...  51 us
    unnamed x25, local copies, waits for them, and re-layouts  11.4 us

profile of v1, /device:TPU:8, one launch (start us, length us, event | category | flops | bytes accessed | tf_op | source)
XLA Modules:
  0.0 63.0 jit_solution(9110058967237598342)
XLA Ops:
  0.6 0.0 copy-start
  0.6 1.0 %copy-done = bf16[2,512,256]{2,1,0:T(8,128)(2,1)S(1)} copy-done((bf16[2,512,256]{2,1,0:T(8,128)(2,1)S(1)}, bf16[2,512,256]{2,1,0:T(8,128)(2,1)}, u32[]{:S(2)}) %copy-start) | copy-done | bytes 524312
  1.7 0.0 copy-start.1
  1.7 1.0 %copy-done.1 = bf16[2,512,256]{2,1,0:T(8,128)(2,1)S(1)} copy-done((bf16[2,512,256]{2,1,0:T(8,128)(2,1)S(1)}, bf16[2,512,256]{2,1,0:T(8,128)(2,1)}, u32[]{:S(2)}) %copy-start.1) | copy-done | bytes 524312
  2.7 0.0 copy-start.2
  2.7 1.0 %copy-done.2 = bf16[2,256,512]{2,1,0:T(8,128)(2,1)S(1)} copy-done((bf16[2,256,512]{2,1,0:T(8,128)(2,1)S(1)}, bf16[2,256,512]{2,1,0:T(8,128)(2,1)}, u32[]{:S(2)}) %copy-start.2) | copy-done | bytes 524312
  3.8 0.0 copy-start.3
  3.8 0.9 %copy-done.3 = f32[2,4,64,64]{3,2,1,0:T(8,128)S(1)} copy-done((f32[2,4,64,64]{3,2,1,0:T(8,128)S(1)}, f32[2,4,64,64]{3,2,1,0:T(8,128)}, u32[]{:S(2)}) %copy-start.3) | copy-done | bytes 131096
  4.7 0.0 copy-start.4
  4.7 0.9 %copy-done.4 = f32[2,4,64,64]{3,2,1,0:T(8,128)S(1)} copy-done((f32[2,4,64,64]{3,2,1,0:T(8,128)S(1)}, f32[2,4,64,64]{3,2,1,0:T(8,128)}, u32[]{:S(2)}) %copy-start.4) | copy-done | bytes 131096
  5.7 0.0 copy-start.5
  5.7 0.9 %copy-done.5 = bf16[2,32,3,256]{3,1,2,0:T(8,128)(2,1)S(1)} copy-done((bf16[2,32,3,256]{3,1,2,0:T(8,128)(2,1)S(1)}, bf16[2,32,3,256]{3,1,2,0:T(8,128)(2,1)}, u32[]{:S(2)}) %copy-start.5) | copy-done | bytes 98328
  6.6 0.0 copy-start.6
  6.6 0.8 %copy-done.6 = f32[2,32,256]{2,1,0:T(8,128)S(1)} copy-done((f32[2,32,256]{2,1,0:T(8,128)S(1)}, f32[2,32,256]{2,1,0:T(8,128)}, u32[]{:S(2)}) %copy-start.6) | copy-done | bytes 65560
  7.4 0.0 copy-start.7
  7.4 0.7 %copy-done.7 = bf16[16,512]{1,0:T(8,128)(2,1)S(1)} copy-done((bf16[16,512]{1,0:T(8,128)(2,1)S(1)}, bf16[16,512]{1,0:T(8,128)(2,1)}, u32[]{:S(2)}) %copy-start.7) | copy-done | bytes 16408
  8.1 0.0 copy-start.8
  8.1 0.7 %copy-done.8 = f32[2,4,256]{2,1,0:T(4,128)S(1)} copy-done((f32[2,4,256]{2,1,0:T(4,128)S(1)}, f32[2,4,256]{2,1,0:T(4,128)}, u32[]{:S(2)}) %copy-start.8) | copy-done | bytes 8216
  8.8 0.0 copy-start.9
  8.8 0.7 %copy-done.9 = f32[2,512]{1,0:T(2,128)S(1)} copy-done((f32[2,512]{1,0:T(2,128)S(1)}, f32[2,512]{1,0:T(2,128)}, u32[]{:S(2)}) %copy-start.9) | copy-done | bytes 4120
  9.5 0.0 copy-start.10
  9.5 0.7 %copy-done.10 = f32[2,256]{1,0:T(2,128)S(1)} copy-done((f32[2,256]{1,0:T(2,128)S(1)}, f32[2,256]{1,0:T(2,128)}, u32[]{:S(2)}) %copy-start.10) | copy-done | bytes 2072
  10.2 51.0 %blocks.1 = (bf16[16,512]{1,0:T(8,128)(2,1)S(1)}, f32[2,32,256]{2,1,0:T(8,128)S(1)}, bf16[2,3,32,256]{3,2,1,0:T(8,128)(2,1)S(1)}) custom-call(bf16[16,512]{1,0:T(8,128)(2,1)S(1)} %copy-done.7, f32[2,32,256]{2,1,0:T(8,128)S(1)} %copy-done.6, bf16[2,3,32,256]{3,2,1,0:T(8,128)(2,1)S(1)} %bitcast.3, f32[2,512]{1,0:T(2,128)S(1)} %copy-done.9, ...), custom_call_target="tpu_custom_call" | custom-call | tf_op jit(solution)/shard_map/blocks/pallas_call | solution.py:278
  61.2 0.6 copy.17
  61.8 0.6 copy.18
  62.4 0.6 %copy.19 = bf16[2,32,3,256]{3,1,2,0:T(8,128)(2,1)} copy(bf16[2,32,3,256]{3,1,2,0:T(8,128)(2,1)S(1)} %bitcast.2) | data formatting | bytes 196608
Async XLA Ops:
  0.6 1.0 %copy-start = (bf16[2,512,256]{2,1,0:T(8,128)(2,1)S(1)}, bf16[2,512,256]{2,1,0:T(8,128)(2,1)}, u32[]{:S(2)}) copy-start(bf16[2,512,256]{2,1,0:T(8,128)(2,1)} %pw_h.1) | copy-start | bytes 1572868
  1.7 1.0 %copy-start.1 = (bf16[2,512,256]{2,1,0:T(8,128)(2,1)S(1)}, bf16[2,512,256]{2,1,0:T(8,128)(2,1)}, u32[]{:S(2)}) copy-start(bf16[2,512,256]{2,1,0:T(8,128)(2,1)} %gw_h.1) | copy-start | bytes 1572868
  2.7 1.0 %copy-start.2 = (bf16[2,256,512]{2,1,0:T(8,128)(2,1)S(1)}, bf16[2,256,512]{2,1,0:T(8,128)(2,1)}, u32[]{:S(2)}) copy-start(bf16[2,256,512]{2,1,0:T(8,128)(2,1)} %ow_h.1) | copy-start | bytes 1572868
  3.8 0.9 %copy-start.3 = (f32[2,4,64,64]{3,2,1,0:T(8,128)S(1)}, f32[2,4,64,64]{3,2,1,0:T(8,128)}, u32[]{:S(2)}) copy-start(f32[2,4,64,64]{3,2,1,0:T(8,128)} %rmap_h.1) | copy-start | bytes 393220
  4.7 0.9 %copy-start.4 = (f32[2,4,64,64]{3,2,1,0:T(8,128)S(1)}, f32[2,4,64,64]{3,2,1,0:T(8,128)}, u32[]{:S(2)}) copy-start(f32[2,4,64,64]{3,2,1,0:T(8,128)} %imap_h.1) | copy-start | bytes 393220
  5.7 0.9 %copy-start.5 = (bf16[2,32,3,256]{3,1,2,0:T(8,128)(2,1)S(1)}, bf16[2,32,3,256]{3,1,2,0:T(8,128)(2,1)}, u32[]{:S(2)}) copy-start(bf16[2,32,3,256]{3,1,2,0:T(8,128)(2,1)} %param.13) | copy-start | bytes 294916
  6.6 0.8 %copy-start.6 = (f32[2,32,256]{2,1,0:T(8,128)S(1)}, f32[2,32,256]{2,1,0:T(8,128)}, u32[]{:S(2)}) copy-start(f32[2,32,256]{2,1,0:T(8,128)} %hid_h.1) | copy-start | bytes 196612
  7.4 0.7 %copy-start.7 = (bf16[16,512]{1,0:T(8,128)(2,1)S(1)}, bf16[16,512]{1,0:T(8,128)(2,1)}, u32[]{:S(2)}) copy-start(bf16[16,512]{1,0:T(8,128)(2,1)} %x_h.1) | copy-start | bytes 49156
  8.1 0.7 %copy-start.8 = (f32[2,4,256]{2,1,0:T(4,128)S(1)}, f32[2,4,256]{2,1,0:T(4,128)}, u32[]{:S(2)}) copy-start(f32[2,4,256]{2,1,0:T(4,128)} %taps_h.1) | copy-start | bytes 24580
  8.8 0.7 %copy-start.9 = (f32[2,512]{1,0:T(2,128)S(1)}, f32[2,512]{1,0:T(2,128)}, u32[]{:S(2)}) copy-start(f32[2,512]{1,0:T(2,128)} %gain_h.1) | copy-start | bytes 12292
  9.5 0.7 %copy-start.10 = (f32[2,256]{1,0:T(2,128)S(1)}, f32[2,256]{1,0:T(2,128)}, u32[]{:S(2)}) copy-start(f32[2,256]{1,0:T(2,128)} %logit_h.1) | copy-start | bytes 6148
